TPU v7x, 32 devices: a whole 2x2x4 slice. The times are simulated.
32 devices in a mesh: fs: 4 (over y, x), tp: 8 (over z, core).
Axes of the slice: x: 2, y: 2, z: 4, core: 2. Of those that a mesh axis runs over, the one named last changes fastest.
Arguments:
- tokens: bfloat16 [4096, 2048], P(('fs', 'tp')), may hold values from -6 to 6
- up_weight: bfloat16 [2048, 4096], P('fs', 'tp'), may hold values from -0.125 to 0.125
- down_weight: bfloat16 [4096, 2048], P('tp', 'fs'), may hold values from -0.09375 to 0.09375
- cotangent: bfloat16 [4096, 2048], P(('fs', 'tp')), may hold values from -6 to 6
Outputs:
- input_grad: bfloat16 [4096, 2048], P(('fs', 'tp'))
- up_grad: float32 [2048, 4096], P('fs', 'tp')
- down_grad: float32 [4096, 2048], P('tp', 'fs')
All inputs are finite; a program needn't handle non-finite values.
Results may differ from a plain program's by a relative error of at most 0.018.
Values may be sent and summed in bfloat16 or wider, within the bound.
A program may use at most 128 MiB of HBM per device.

v0:
```python
import jax
import jax.numpy as jnp
from jax import lax
from jax.sharding import PartitionSpec as P


def shards(tokens, up_weight, down_weight, cotangent):
    rows_all, cot_all = (
        lax.all_gather(tokens, "tp", axis=0, tiled=True),
        lax.all_gather(cotangent, "tp", axis=0, tiled=True),
    )
    up_whole = lax.all_gather(up_weight, "fs", axis=0, tiled=True)
    pre = jnp.dot(rows_all, up_whole, preferred_element_type=jnp.float32)
    active = jnp.maximum(pre, 0.0)
    hidden = (active * active).astype(jnp.bfloat16)
    part = cot_all
    dhidden = lax.dot_general(
        part,
        lax.all_gather(down_weight, "fs", axis=1, tiled=True),
        (((1,), (1,)), ((), ())),
        preferred_element_type=jnp.float32,
    )
    dpre = (2.0 * active * dhidden).astype(jnp.bfloat16)
    count_all = tokens.shape[0] * lax.axis_size("fs") * lax.axis_size("tp")
    factor = 1.0 / jnp.sqrt(jnp.float32(count_all))
    part = rows_all
    up_grad = (
        lax.psum_scatter(
            lax.dot_general(
                part, dpre, (((0,), (0,)), ((), ())), preferred_element_type=jnp.float32
            ).astype(jnp.bfloat16),
            "fs",
            scatter_dimension=0,
            tiled=True,
        ).astype(jnp.float32)
        * factor
    )
    down_term = lax.dot_general(
        hidden, cot_all, (((0,), (0,)), ((), ())), preferred_element_type=jnp.float32
    )
    down_grad = (
        lax.psum_scatter(
            down_term.astype(jnp.bfloat16), "fs", scatter_dimension=1, tiled=True
        ).astype(jnp.float32)
        * factor
    )
    part = dpre
    prod = lax.dot_general(
        part, up_whole, (((1,), (1,)), ((), ())), preferred_element_type=jnp.float32
    )
    rounded = lax.optimization_barrier(prod.astype(jnp.bfloat16))
    grad_rows = lax.psum_scatter(
        rounded.astype(jnp.float32).astype(jnp.bfloat16), "tp", scatter_dimension=0, tiled=True
    )
    return (grad_rows, up_grad, down_grad)


def solution(mesh):
    placed = (P(("fs", "tp"), None), P("fs", "tp"), P("tp", "fs"), P(("fs", "tp"), None))
    return jax.shard_map(
        shards,
        mesh=mesh,
        in_specs=placed,
        out_specs=(P(("fs", "tp"), None), P("fs", "tp"), P("tp", "fs")),
        check_vma=False,
    )
```

profile of v0, /device:TPU:0, one launch (start us, length us, event | category | flops | bytes accessed | tf_op | source)
XLA Modules:
  0.0 314.8 jit_solution(16396900336464673650)
XLA Ops:
  7.2 0.0 all-gather.7.cloned.1.call-start
  7.2 0.7 all-gather.7.cloned.1.call-update
  7.9 0.0 all-gather.5.cloned.1.call-start
  7.9 0.7 all-gather.5.cloned.1.call-update
  8.6 0.0 all-gather.9.cloned.1.call-start
  8.7 0.7 all-gather.9.cloned.1.call-update
  9.4 0.0 all-gather.11.cloned.1.call-start
  9.4 0.5 all-gather.11.cloned.1.call-update
  10.0 0.0 reduce-scatter.8.cloned.1.call-start
  10.0 37.7 %all-gather.7.cloned.1.call-done = bf16[2048,512]{1,0:T(8,128)(2,1)} async-done(((bf16[512,512]{1,0:T(8,128)(2,1)}), bf16[2048,512]{1,0:T(8,128)(2,1)}) %all-gather.7.cloned.1.call-update) | async-done | bytes 2097168 | tf_op jit(solution)/shard_map/all_gather | solution.py:12
  47.8 48.5 %all-gather.5.cloned.1.call-done = bf16[1024,2048]{1,0:T(8,128)(2,1)} async-done(((bf16[128,2048]{1,0:T(8,128)(2,1)}), bf16[1024,2048]{1,0:T(8,128)(2,1)}) %all-gather.5.cloned.1.call-update) | async-done | bytes 4194320 | tf_op jit(solution)/shard_map/all_gather | solution.py:9
  96.2 5.2 %fusion.3 = f32[1024,512]{1,0:T(8,128)S(1)} fusion(bf16[1024,2048]{1,0:T(8,128)(2,1)} %all-gather.5.cloned.1.call-done, bf16[2048,512]{1,0:T(8,128)(2,1)} %all-gather.7.cloned.1.call-done), kind=kOutput, calls=%fused_computation.10 | convolution fusion | flops 2147483648 | bytes 8388608 | tf_op jit(solution)/shard_map/dot_general | solution.py:13
  101.4 42.1 %all-gather.9.cloned.1.call-done = bf16[1024,2048]{1,0:T(8,128)(2,1)} async-done(((bf16[128,2048]{1,0:T(8,128)(2,1)}), bf16[1024,2048]{1,0:T(8,128)(2,1)}) %all-gather.9.cloned.1.call-update) | async-done | bytes 4194320 | tf_op jit(solution)/shard_map/all_gather | solution.py:10
  143.6 5.9 %convolution_convert_fusion.1 = bf16[512,2048]{0,1:T(8,128)(2,1)} fusion(bf16[1024,2048]{1,0:T(8,128)(2,1)} %all-gather.9.cloned.1.call-done, f32[1024,512]{1,0:T(8,128)S(1)} %fusion.3), kind=kOutput, calls=%fused_computation.1 | convolution fusion | flops 2150105088 | bytes 8388608 | tf_op jit(solution)/shard_map/dot_general | solution.py:38
  149.5 0.0 reduce-scatter.8.cloned.1.call-update
  149.5 0.0 reduce-scatter.6.cloned.1.call-start
  149.5 29.6 %all-gather.11.cloned.1.call-done = bf16[512,2048]{1,0:T(8,128)(2,1)} async-done(((bf16[512,512]{1,0:T(8,128)(2,1)}), bf16[512,2048]{1,0:T(8,128)(2,1)}) %all-gather.11.cloned.1.call-update) | async-done | bytes 2097168 | tf_op jit(solution)/shard_map/all_gather | solution.py:19
  179.1 5.4 %multiply_convert_fusion.1 = bf16[1024,512]{1,0:T(8,128)(2,1)S(1)} fusion(f32[1024,512]{1,0:T(8,128)S(1)} %fusion.3, bf16[1024,2048]{1,0:T(8,128)(2,1)} %all-gather.9.cloned.1.call-done, bf16[512,2048]{1,0:T(8,128)(2,1)} %all-gather.11.cloned.1.call-done), kind=kOutput, calls=%fused_computation.5 | convolution fusion | flops 2149580800 | bytes 9437184 | tf_op jit(solution)/shard_map/dot_general | solution.py:17
  184.5 0.0 copy-done
  184.5 3.7 %fusion = bf16[2048,512]{0,1:T(8,128)(2,1)} fusion(bf16[1024,512]{1,0:T(8,128)(2,1)S(1)} %multiply_convert_fusion.1, bf16[1024,2048]{1,0:T(8,128)(2,1)S(1)} %copy-done), kind=kOutput, calls=%fused_computation.3 | convolution fusion | flops 2148532224 | bytes 7340032 | tf_op jit(solution)/shard_map/dot_general | solution.py:29
  188.2 0.0 reduce-scatter.6.cloned.1.call-update
  188.2 0.0 reduce-scatter.4.cloned.1.call-start
  188.3 1.6 copy-done.1
  189.9 4.3 %convolution_convert_fusion = bf16[1024,2048]{1,0:T(8,128)(2,1)} fusion(bf16[1024,512]{1,0:T(8,128)(2,1)S(1)} %multiply_convert_fusion.1, bf16[2048,512]{1,0:T(8,128)(2,1)S(1)} %copy-done.1), kind=kOutput, calls=%fused_computation | convolution fusion | flops 2149580800 | bytes 7340032 | tf_op jit(solution)/shard_map/dot_general | solution.py:48
  194.2 0.0 reduce-scatter.4.cloned.1.call-update
  194.2 23.0 %reduce-scatter.8.cloned.1.call-done = bf16[512,512]{0,1:T(8,128)(2,1)} async-done(((bf16[512,2048]{0,1:T(8,128)(2,1)}), bf16[512,512]{0,1:T(8,128)(2,1)}) %reduce-scatter.8.cloned.1.call-update) | async-done | bytes 524304 | tf_op jit(solution)/shard_map/reduce_scatter | solution.py:42
  217.1 1.2 convert_multiply_fusion
  218.3 1.3 copy.9
  219.6 35.5 %reduce-scatter.6.cloned.1.call-done = bf16[512,512]{0,1:T(8,128)(2,1)} async-done(((bf16[2048,512]{0,1:T(8,128)(2,1)}), bf16[512,512]{0,1:T(8,128)(2,1)}) %reduce-scatter.6.cloned.1.call-update) | async-done | bytes 524304 | tf_op jit(solution)/shard_map/reduce_scatter | solution.py:28
  255.2 1.2 convert_multiply_fusion.1
  256.4 1.3 copy.8
  257.7 50.3 %reduce-scatter.4.cloned.1.call-done = bf16[128,2048]{1,0:T(8,128)(2,1)} async-done(((bf16[1024,2048]{1,0:T(8,128)(2,1)}), bf16[128,2048]{1,0:T(8,128)(2,1)}) %reduce-scatter.4.cloned.1.call-update) | async-done | bytes 524304 | tf_op jit(solution)/shard_map/reduce_scatter | solution.py:52
  (2 shorter events, 0.0 us)
Async XLA Ops:
  7.2 40.6 %all-gather.7.cloned.1.call-start = ((), (), s32[]{:S(2)}) async-start(), calls=%async_computation.4 | async-start | bytes 2621440 | tf_op jit(solution)/shard_map/all_gather | solution.py:12
  7.9 88.3 %all-gather.5.cloned.1.call-start = ((), (), s32[]{:S(2)}) async-start(), calls=%async_computation.3 | async-start | bytes 4718592 | tf_op jit(solution)/shard_map/all_gather | solution.py:9
  8.6 134.9 %all-gather.9.cloned.1.call-start = ((), (), s32[]{:S(2)}) async-start(), calls=%async_computation.5 | async-start | bytes 4718592 | tf_op jit(solution)/shard_map/all_gather | solution.py:10
  9.4 169.7 %all-gather.11.cloned.1.call-start = ((), (), s32[]{:S(2)}) async-start(), calls=%async_computation.6 | async-start | bytes 2621440 | tf_op jit(solution)/shard_map/all_gather | solution.py:19
  10.0 207.2 %reduce-scatter.8.cloned.1.call-start = ((), (), s32[]{:S(2)}) async-start(), calls=%async_computation.9 | async-start | bytes 2621440 | tf_op jit(solution)/shard_map/reduce_scatter | solution.py:42
  149.5 105.7 %reduce-scatter.6.cloned.1.call-start = ((), (), s32[]{:S(2)}) async-start(), calls=%async_computation.8 | async-start | bytes 2621440 | tf_op jit(solution)/shard_map/reduce_scatter | solution.py:28
  179.1 5.4 %copy-start = (bf16[1024,2048]{1,0:T(8,128)(2,1)S(1)}, bf16[1024,2048]{1,0:T(8,128)(2,1)}, u32[]{:S(2)}) copy-start(bf16[1024,2048]{1,0:T(8,128)(2,1)} %all-gather.5.cloned.1.call-done) | copy-start | bytes 12582916
  188.2 1.6 copy-start.1
  188.2 119.7 %reduce-scatter.4.cloned.1.call-start = ((), (), s32[]{:S(2)}) async-start(), calls=%async_computation.7 | async-start | bytes 4718592 | tf_op jit(solution)/shard_map/reduce_scatter | solution.py:52
Sparse Core Ops, SparseCore 0:
  9.8 37.8 all-gather.6
  49.3 46.8 all-gather.4
  97.8 45.6 all-gather.8
  145.2 33.8 all-gather.10
  181.9 35.1 reduce-scatter.7
  220.0 35.1 reduce-scatter.5
  258.0 49.8 reduce-scatter.3
where the time goes:
time: 315 us
  waiting for transfers between devices  269 us (85%)
  matrix products  24.5 us (8%)
  between operations  14.2 us (5%)
  local copies, waits for them, and re-layouts  4.18 us (1%)
    reduce_scatter x1, waiting for transfers between devices, shards(): lax.psum_scatter(rounded.astype(jnp.float32).astype(jnp.bfloat16), 'tp',...  50.3 us
    all_gather x1, waiting for transfers between devices, shards(): lax.all_gather(tokens, 'tp', axis=0, tiled=True)  48.5 us
    all_gather x1, waiting for transfers between devices, shards(): lax.all_gather(cotangent, 'tp', axis=0, tiled=True)  42.1 us
    all_gather x1, waiting for transfers between devices, shards(): up_whole = lax.all_gather(up_weight, 'fs', axis=0, tiled=True)  37.7 us
    reduce_scatter x1, waiting for transfers between devices, shards(): lax.psum_scatter(lax.dot_general(part, dpre, (((0,), (0,)), ((), ())), pr...  35.5 us
    all_gather x1, waiting for transfers between devices, shards(): lax.all_gather(down_weight, 'fs', axis=1, tiled=True)  29.6 us
    reduce_scatter x1, waiting for transfers between devices, shards(): lax.psum_scatter(down_term.astype(jnp.bfloat16), 'fs', scatter_dimension=...  23 us
  transfers between devices with their start and end apart: 7, of which 7 were waited for; matrix products, arithmetic and copies ran while one was open for 9% of the time, Pallas kernels for 0%

commit v1 on v0

--- a/solution.py
+++ b/solution.py
@@ -2,6 +2,21 @@
 import jax.numpy as jnp
 from jax import lax
 from jax.sharding import PartitionSpec as P
+
+
+def cover_the_units(shard_in, in_dim):
+    sheets = []
+    size_here = lax.psum(1, axis_name="fs")
+    for dd in tuple(range(size_here)):
+        sheets.append((dd, (dd + 1) % size_here))
+    res = [None] * size_here
+    res[size_here - 1] = shard_in
+    for ii in range(size_here - 2, -1, -1):
+        res[ii] = lax.ppermute(res[ii + 1], axis_name="fs", perm=sheets)
+    raw_out = jnp.roll(
+        jnp.concatenate(res, in_dim), (lax.axis_index("fs") + 1) * shard_in.shape[in_dim], in_dim
+    )
+    return raw_out
 
 
 def shards(tokens, up_weight, down_weight, cotangent):
@@ -9,7 +24,7 @@
         lax.all_gather(tokens, "tp", axis=0, tiled=True),
         lax.all_gather(cotangent, "tp", axis=0, tiled=True),
     )
-    up_whole = lax.all_gather(up_weight, "fs", axis=0, tiled=True)
+    up_whole = cover_the_units(up_weight, 0)
     pre = jnp.dot(rows_all, up_whole, preferred_element_type=jnp.float32)
     active = jnp.maximum(pre, 0.0)
     hidden = (active * active).astype(jnp.bfloat16)

time: 315 us -> 285 us (0.905)
  waiting for transfers between devices: 269 us -> 228 us
  local copies, waits for them, and re-layouts: 4.18 us -> 9.33 us
  starting transfers between devices: 0.27 us -> 4.22 us
    all_gather x1, waiting for transfers between devices: 48.5 us -> 0.01 us  [shards(): lax.all_gather(tokens, 'tp', axis=0, tiled=True)]
    ppermute x0 -> x3, waiting for transfers between devices: none -> 39.7 us  [cover_the_units(): res[ii] = lax.ppermute(res[ii + 1], axis_name='fs', perm=sheets)]
    all_gather x1 -> x0, waiting for transfers between devices: 37.7 us -> none  [shards(): up_whole = lax.all_gather(up_weight, 'fs', axis=0, tiled=True)]
    reduce_scatter x1, waiting for transfers between devices: 35.5 us -> 21.9 us  [shards(): lax.psum_scatter(lax.dot_general(part, dpre, (((0,), (0,)), ((), ())), pr...]
    reduce_scatter x1, waiting for transfers between devices: 23 us -> 35.6 us  [shards(): lax.psum_scatter(down_term.astype(jnp.bfloat16), 'fs', scatter_dimension=...]
    all_gather x1, waiting for transfers between devices: 42.1 us -> 48.5 us  [shards(): lax.all_gather(cotangent, 'tp', axis=0, tiled=True)]
    unnamed x6 -> x13, local copies, waits for them, and re-layouts: 4.18 us -> 8.5 us
    ppermute x0 -> x3, starting transfers between devices: none -> 3.81 us  [cover_the_units(): res[ii] = lax.ppermute(res[ii + 1], axis_name='fs', perm=sheets)]
  transfers between devices with their start and end apart: 7 -> 9, of which waited for: 7 -> 8; matrix products, arithmetic and copies ran while one was open for 9% -> 10% of each run, Pallas kernels for 0% -> 0%
where the time goes in v1:
time: 285 us; the launch traced here: 284 us
  waiting for transfers between devices  228 us (80%)
  matrix products  26.2 us (9%)
  between operations  14.2 us (5%)
  local copies, waits for them, and re-layouts  9.33 us (3%)
  starting transfers between devices  4.22 us (1%)
    reduce_scatter x1, waiting for transfers between devices, shards(): lax.psum_scatter(rounded.astype(jnp.float32).astype(jnp.bfloat16), 'tp',...  50.2 us
    all_gather x1, waiting for transfers between devices, shards(): lax.all_gather(cotangent, 'tp', axis=0, tiled=True)  48.5 us
    ppermute x3, waiting for transfers between devices, cover_the_units(): res[ii] = lax.ppermute(res[ii + 1], axis_name='fs', perm=sheets)  39.7 us
    reduce_scatter x1, waiting for transfers between devices, shards(): lax.psum_scatter(down_term.astype(jnp.bfloat16), 'fs', scatter_dimension=...  35.6 us
    all_gather x1, waiting for transfers between devices, shards(): lax.all_gather(down_weight, 'fs', axis=1, tiled=True)  30 us
    reduce_scatter x1, waiting for transfers between devices, shards(): lax.psum_scatter(lax.dot_general(part, dpre, (((0,), (0,)), ((), ())), pr...  21.9 us
    unnamed x13, local copies, waits for them, and re-layouts  8.5 us
    dot_general x1, matrix products, shards(): lax.dot_general(part, up_whole, (((1,), (1,)), ((), ())), preferred_eleme...  5.94 us
  transfers between devices with their start and end apart: 9, of which 8 were waited for; matrix products, arithmetic and copies ran while one was open for 10% of the time, Pallas kernels for 0%

profile of v1, /device:TPU:0, one launch (start us, length us, event | category | flops | bytes accessed | tf_op | source)
XLA Modules:
  0.0 284.2 jit_solution(1944741191144420966)
XLA Ops:
  7.2 0.7 all-gather.4.cloned.1.call-update
  8.0 0.7 all-gather.8.cloned.1.call-update
  8.7 0.7 all-gather.6.cloned.1.call-update
  9.4 3.0 %collective-permute-start = (bf16[512,512]{1,0:T(8,128)(2,1)}, bf16[512,512]{1,0:T(8,128)(2,1)S(1)}, u32[]{:S(2)}, u32[]{:S(2)}) collective-permute-start(bf16[512,512]{1,0:T(8,128)(2,1)} %param.5), channel_id=1, source_target_pairs={{0,8},{8,16},{16,24},{24,0},{1,9},{9,17},{17,25},{25,1},{2,10},{10... | collective-permute-start | bytes 1572872 | tf_op jit(solution)/shard_map/ppermute | solution.py:15
  12.5 13.1 %collective-permute-done = bf16[512,512]{1,0:T(8,128)(2,1)S(1)} collective-permute-done((bf16[512,512]{1,0:T(8,128)(2,1)}, bf16[512,512]{1,0:T(8,128)(2,1)S(1)}, u32[]{:S(2)}, u32[]{:S(2)}) %collective-permute-start) | collective-permute-done | bytes 524320 | tf_op jit(solution)/shard_map/ppermute | solution.py:15
  25.5 0.8 collective-permute-start.1
  26.3 13.3 %collective-permute-done.1 = bf16[512,512]{1,0:T(8,128)(2,1)S(1)} collective-permute-done((bf16[512,512]{1,0:T(8,128)(2,1)S(1)}, bf16[512,512]{1,0:T(8,128)(2,1)S(1)}, u32[]{:S(2)}, u32[]{:S(2)}) %collective-permute-start.1) | collective-permute-done | bytes 524320 | tf_op jit(solution)/shard_map/ppermute | solution.py:15
  39.6 13.3 %collective-permute-done.2 = bf16[512,512]{1,0:T(8,128)(2,1)S(1)} collective-permute-done((bf16[512,512]{1,0:T(8,128)(2,1)S(1)}, bf16[512,512]{1,0:T(8,128)(2,1)S(1)}, u32[]{:S(2)}, u32[]{:S(2)}) %collective-permute-start.2) | collective-permute-done | bytes 524320 | tf_op jit(solution)/shard_map/ppermute | solution.py:15
  53.0 0.9 constant_dynamic-update-slice_fusion.7
  53.8 0.9 constant_dynamic-update-slice_fusion.6
  54.7 0.8 constant_dynamic-update-slice_fusion.5
  55.5 0.8 constant_dynamic-update-slice_fusion.4
  56.4 0.8 constant_dynamic-update-slice_fusion.3
  57.2 0.8 constant_dynamic-update-slice_fusion.2
  58.0 0.8 constant_dynamic-update-slice_fusion.1
  58.9 0.8 constant_dynamic-update-slice_fusion
  59.7 5.2 %fusion.3 = f32[512,1024]{1,0:T(8,128)S(1)} fusion(bf16[1024,2048]{1,0:T(8,128)(2,1)} %all-gather.4.cloned.1.call-done, bf16[4096,512]{1,0:T(8,128)(2,1)} %constant_dynamic-update-slice_fusion, s32[]{:T(128)S(6)} %select_n.14), kind=kOutput, calls=%fused_computation.8 | convolution fusion | flops 2147483648 | bytes 8388612 | tf_op jit(solution)/shard_map/dot_general | solution.py:28
  64.9 30.0 %all-gather.8.cloned.1.call-done = bf16[512,2048]{1,0:T(8,128)(2,1)} async-done(((bf16[512,512]{1,0:T(8,128)(2,1)}), bf16[512,2048]{1,0:T(8,128)(2,1)}) %all-gather.8.cloned.1.call-update) | async-done | bytes 2097168 | tf_op jit(solution)/shard_map/all_gather | solution.py:34
  94.9 48.5 %all-gather.6.cloned.1.call-done = bf16[1024,2048]{1,0:T(8,128)(2,1)} async-done(((bf16[128,2048]{1,0:T(8,128)(2,1)}), bf16[1024,2048]{1,0:T(8,128)(2,1)}) %all-gather.6.cloned.1.call-update) | async-done | bytes 4194320 | tf_op jit(solution)/shard_map/all_gather | solution.py:25
  143.4 5.4 %fusion.1 = bf16[1024,512]{0,1:T(8,128)(2,1)S(1)} fusion(f32[512,1024]{1,0:T(8,128)S(1)} %fusion.3, bf16[1024,2048]{1,0:T(8,128)(2,1)} %all-gather.6.cloned.1.call-done, bf16[512,2048]{1,0:T(8,128)(2,1)} %all-gather.8.cloned.1.call-done), kind=kOutput, calls=%fused_computation.5 | convolution fusion | flops 2149580800 | bytes 9437184 | tf_op jit(solution)/shard_map/dot_general | solution.py:32
  148.8 3.7 %fusion = bf16[2048,512]{0,1:T(8,128)(2,1)} fusion(bf16[1024,512]{0,1:T(8,128)(2,1)S(1)} %fusion.1, bf16[1024,2048]{1,0:T(8,128)(2,1)S(1)} %copy-done.1), kind=kOutput, calls=%fused_computation.3 | convolution fusion | flops 2148532224 | bytes 7340032 | tf_op jit(solution)/shard_map/dot_general | solution.py:44
  152.6 0.0 reduce-scatter.8.cloned.1.call-start
  152.6 5.9 %convolution_convert_fusion.1 = bf16[512,2048]{0,1:T(8,128)(2,1)} fusion(bf16[1024,2048]{1,0:T(8,128)(2,1)} %all-gather.6.cloned.1.call-done, f32[512,1024]{1,0:T(8,128)S(1)} %fusion.3), kind=kOutput, calls=%fused_computation.1 | convolution fusion | flops 2150105088 | bytes 8388608 | tf_op jit(solution)/shard_map/dot_general | solution.py:53
  158.5 0.2 reduce-scatter.4.cloned.1.call-start
  158.8 5.9 %convolution_convert_fusion = bf16[1024,2048]{1,0:T(8,128)(2,1)} fusion(bf16[1024,512]{0,1:T(8,128)(2,1)S(1)} %fusion.1, bf16[4096,512]{1,0:T(8,128)(2,1)} %constant_dynamic-update-slice_fusion, s32[]{:T(128)S(6)} %select_n.14), kind=kOutput, calls=%fused_computation | convolution fusion | flops 2149580800 | bytes 7340036 | tf_op jit(solution)/shard_map/dot_general | solution.py:63
  164.7 21.9 %reduce-scatter.6.cloned.1.call-done = bf16[512,512]{0,1:T(8,128)(2,1)} async-done(((bf16[2048,512]{0,1:T(8,128)(2,1)}), bf16[512,512]{0,1:T(8,128)(2,1)}) %reduce-scatter.6.cloned.1.call-update) | async-done | bytes 524304 | tf_op jit(solution)/shard_map/reduce_scatter | solution.py:43
  186.7 1.2 convert_multiply_fusion.1
  187.9 1.3 copy.9
  189.2 35.6 %reduce-scatter.8.cloned.1.call-done = bf16[512,512]{0,1:T(8,128)(2,1)} async-done(((bf16[512,2048]{0,1:T(8,128)(2,1)}), bf16[512,512]{0,1:T(8,128)(2,1)}) %reduce-scatter.8.cloned.1.call-update) | async-done | bytes 524304 | tf_op jit(solution)/shard_map/reduce_scatter | solution.py:57
  224.7 1.2 convert_multiply_fusion
  225.9 1.3 copy.10
  227.2 50.2 %reduce-scatter.4.cloned.1.call-done = bf16[128,2048]{1,0:T(8,128)(2,1)} async-done(((bf16[1024,2048]{1,0:T(8,128)(2,1)}), bf16[128,2048]{1,0:T(8,128)(2,1)}) %reduce-scatter.4.cloned.1.call-update) | async-done | bytes 524304 | tf_op jit(solution)/shard_map/reduce_scatter | solution.py:67
  (13 shorter events, 0.2 us)
Async XLA Ops:
  7.2 48.4 %copy-start = (bf16[512,512]{1,0:T(8,128)(2,1)S(1)}, bf16[512,512]{1,0:T(8,128)(2,1)}, u32[]{:S(2)}) copy-start(bf16[512,512]{1,0:T(8,128)(2,1)} %param.5) | copy-start | bytes 1572868
  7.2 52.5 %all-gather.4.cloned.1.call-start = ((), (), s32[]{:S(2)}) async-start(), calls=%async_computation.3 | async-start | bytes 4718592 | tf_op jit(solution)/shard_map/all_gather | solution.py:24
  7.9 87.0 %all-gather.8.cloned.1.call-start = ((), (), s32[]{:S(2)}) async-start(), calls=%async_computation.5 | async-start | bytes 2621440 | tf_op jit(solution)/shard_map/all_gather | solution.py:34
  8.7 134.8 %all-gather.6.cloned.1.call-start = ((), (), s32[]{:S(2)}) async-start(), calls=%async_computation.4 | async-start | bytes 4718592 | tf_op jit(solution)/shard_map/all_gather | solution.py:25
  9.4 177.3 %reduce-scatter.6.cloned.1.call-start = ((), (), s32[]{:S(2)}) async-start(), calls=%async_computation.7 | async-start | bytes 2621440 | tf_op jit(solution)/shard_map/reduce_scatter | solution.py:43
  9.4 16.1 %collective-permute-start = (bf16[512,512]{1,0:T(8,128)(2,1)}, bf16[512,512]{1,0:T(8,128)(2,1)S(1)}, u32[]{:S(2)}, u32[]{:S(2)}) collective-permute-start(bf16[512,512]{1,0:T(8,128)(2,1)} %param.5), channel_id=1, source_target_pairs={{0,8},{8,16},{16,24},{24,0},{1,9},{9,17},{17,25},{25,1},{2,10},{10... | collective-permute-start | bytes 1572872 | tf_op jit(solution)/shard_map/ppermute | solution.py:15
  25.5 14.1 %collective-permute-start.1 = (bf16[512,512]{1,0:T(8,128)(2,1)S(1)}, bf16[512,512]{1,0:T(8,128)(2,1)S(1)}, u32[]{:S(2)}, u32[]{:S(2)}) collective-permute-start(bf16[512,512]{1,0:T(8,128)(2,1)S(1)} %collective-permute-done), channel_id=1, source_target_pairs={{0,8},{8,16},{16,24},{24,0},{1,9},{9,17},{17,25},{25,1},{2,10},{10... | collective-permute-start | bytes 1572872 | tf_op jit(solution)/shard_map/ppermute | solution.py:15
  39.6 13.3 %collective-permute-start.2 = (bf16[512,512]{1,0:T(8,128)(2,1)S(1)}, bf16[512,512]{1,0:T(8,128)(2,1)S(1)}, u32[]{:S(2)}, u32[]{:S(2)}) collective-permute-start(bf16[512,512]{1,0:T(8,128)(2,1)S(1)} %collective-permute-done.1), channel_id=1, source_target_pairs={{0,8},{8,16},{16,24},{24,0},{1,9},{9,17},{17,25},{25,1},{2,10},{10... | collective-permute-start | bytes 1572872 | tf_op jit(solution)/shard_map/ppermute | solution.py:15
  143.4 5.4 %copy-start.1 = (bf16[1024,2048]{1,0:T(8,128)(2,1)S(1)}, bf16[1024,2048]{1,0:T(8,128)(2,1)}, u32[]{:S(2)}) copy-start(bf16[1024,2048]{1,0:T(8,128)(2,1)} %all-gather.4.cloned.1.call-done) | copy-start | bytes 12582916
  152.6 72.2 %reduce-scatter.8.cloned.1.call-start = ((), (), s32[]{:S(2)}) async-start(), calls=%async_computation.8 | async-start | bytes 2621440 | tf_op jit(solution)/shard_map/reduce_scatter | solution.py:57
  158.5 118.9 %reduce-scatter.4.cloned.1.call-start = ((), (), s32[]{:S(2)}) async-start(), calls=%async_computation.6 | async-start | bytes 4718592 | tf_op jit(solution)/shard_map/reduce_scatter | solution.py:67
Sparse Core Ops, SparseCore 0:
  9.6 49.5 all-gather.3
  61.0 33.8 all-gather.7
  96.5 46.8 all-gather.5
  152.7 33.9 reduce-scatter.5
  189.5 35.1 reduce-scatter.7
  227.5 49.8 reduce-scatter.3
